TPU v7x, 32 devices: a whole 2x2x4 slice. The times are simulated.
32 devices in a mesh: kv: 8 (over z, y), tp: 4 (over x, core).
Axes of the slice: x: 2, y: 2, z: 4, core: 2. Of those that a mesh axis runs over, the one named last changes fastest.
Arguments:
- tokens: bfloat16 [256, 4096], P(None, ('kv', 'tp')), may hold values from -60 to 60
- past_state: float32 [256, 16, 128, 128], P('kv', 'tp'), may hold values from -4 to 4
- pre_gain: float32 [4096], replicated, may hold values from 0.1 to 1.9
- pre_gate: bfloat16 [4096, 11264], P(None, ('kv', 'tp')), may hold values from -0.09375 to 0.09375
- pre_up: bfloat16 [4096, 11264], P(None, ('kv', 'tp')), may hold values from -0.09375 to 0.09375
- pre_down: bfloat16 [11264, 4096], P(('kv', 'tp')), may hold values from -0.109375 to 0.109375
- mix_gain: float32 [4096], replicated, may hold values from 0.1 to 1.9
- query_weight: bfloat16 [4096, 2048], P('kv', 'tp'), may hold values from -0.09375 to 0.09375
- forget_weight: bfloat16 [4096, 2048], P('kv', 'tp'), may hold values from -0.09375 to 0.09375
- value_weight: bfloat16 [4096, 2048], P('kv', 'tp'), may hold values from -0.09375 to 0.09375
- output_gate_weight: bfloat16 [4096, 2048], P('kv', 'tp'), may hold values from -0.09375 to 0.09375
- forget_floor: float32 [2048], P('tp'), may hold values from 0.02 to 0.9
- head_gain: float32 [128], replicated, may hold values from 0.1 to 1.9
- proj_out: bfloat16 [2048, 4096], P('tp', 'kv'), may hold values from -0.125 to 0.125
- post_gain: float32 [4096], replicated, may hold values from 0.1 to 1.9
- post_gate: bfloat16 [4096, 11264], P(None, ('kv', 'tp')), may hold values from -0.09375 to 0.09375
- post_up: bfloat16 [4096, 11264], P(None, ('kv', 'tp')), may hold values from -0.09375 to 0.09375
- post_down: bfloat16 [11264, 4096], P(('kv', 'tp')), may hold values from -0.109375 to 0.109375
Outputs:
- result: bfloat16 [256, 4096], P(None, ('kv', 'tp'))
- new_state: float32 [256, 16, 128, 128], P('kv', 'tp')
All inputs are finite; a program needn't handle non-finite values.
Results may differ from a plain program's by a relative error of at most 0.014.
Values may be sent and summed in bfloat16 or wider, within the bound.
A program may use at most 128 MiB of HBM per device.

v0:
```python
import jax
import jax.numpy as jnp
from jax import lax
from jax.sharding import PartitionSpec as P

D = 4096
epsilon = 1e-06


def half_inputs(activations, gain, w_gate, w_up):
    piece_float = lax.all_gather(activations, ("kv", "tp"), axis=1, tiled=True).astype(jnp.float32)
    normed = (piece_float * gain).astype(jnp.bfloat16)
    gate_acc = jnp.dot(normed, w_gate, preferred_element_type=jnp.float32)
    up_acc = jnp.dot(normed, w_up, preferred_element_type=jnp.float32)
    squares = jnp.sum(piece_float * piece_float, axis=1)
    row_scale = lax.rsqrt(squares / D + epsilon)[:, None]
    return (jax.nn.silu(row_scale * gate_acc) * (row_scale * up_acc)).astype(jnp.bfloat16)


def down_sum(hidden, w_down):
    return lax.psum_scatter(
        jnp.dot(hidden, w_down, preferred_element_type=jnp.float32),
        ("kv", "tp"),
        scatter_dimension=1,
        tiled=True,
    )


def per_device(
    tokens,
    past_state,
    pre_gain,
    pre_gate,
    pre_up,
    pre_down,
    mix_gain,
    query_weight,
    forget_weight,
    value_weight,
    output_gate_weight,
    forget_floor,
    head_gain,
    proj_out,
    post_gain,
    post_gate,
    post_up,
    post_down,
):
    whole_rows = lax.all_gather(tokens, ("kv", "tp"), axis=1, tiled=True)
    whole_float = whole_rows.astype(jnp.float32)
    row_scale = lax.rsqrt(jnp.mean(whole_float * whole_float, axis=1, keepdims=True) + epsilon)
    normed = (whole_float * pre_gain).astype(jnp.bfloat16)
    gate_pre = row_scale * jnp.dot(normed, pre_gate, preferred_element_type=jnp.float32)
    up_pre = row_scale * jnp.dot(normed, pre_up, preferred_element_type=jnp.float32)
    hidden = (jax.nn.silu(gate_pre) * up_pre).astype(jnp.bfloat16)
    kv_sums = lax.psum_scatter(
        jnp.dot(hidden, pre_down, preferred_element_type=jnp.float32).astype(jnp.bfloat16),
        "kv",
        scatter_dimension=1,
        tiled=True,
    )
    block_sum = lax.psum(kv_sums, "tp").astype(jnp.float32)
    block_width = block_sum.shape[1]
    block_old = lax.dynamic_slice_in_dim(
        whole_rows, lax.axis_index("kv") * block_width, block_width, 1
    )
    block_rows = (block_old.astype(jnp.float32) + 0.5 * block_sum).astype(jnp.bfloat16)
    own_width = block_width // lax.axis_size("tp")
    after_first = lax.dynamic_slice_in_dim(
        block_rows, lax.axis_index("tp") * own_width, own_width, 1
    )
    block_width = block_rows.shape[1]
    block_float = block_rows.astype(jnp.float32)
    block_gain = lax.dynamic_slice_in_dim(
        mix_gain, lax.axis_index("kv") * block_width, block_width, 0
    )
    squares = lax.psum(jnp.sum(block_float * block_float, axis=1), "kv")
    normed = (block_float * block_gain).astype(jnp.bfloat16)
    own_rows = past_state.shape[0]
    weight_list = (query_weight, forget_weight, value_weight, output_gate_weight)
    projected = lax.psum_scatter(
        jnp.concatenate(
            [
                jnp.dot(normed, weight_part, preferred_element_type=jnp.float32)
                for weight_part in weight_list
            ],
            axis=1,
        ).astype(jnp.bfloat16),
        "kv",
        scatter_dimension=0,
        tiled=True,
    ).astype(jnp.float32)
    own_squares = lax.dynamic_slice_in_dim(squares, lax.axis_index("kv") * own_rows, own_rows, 0)
    projected = projected * lax.rsqrt(own_squares / D + epsilon)[:, None]
    pre_query, pre_forget, pre_value, pre_gate_out = jnp.split(projected, 4, axis=1)
    local_heads = past_state.shape[1]
    head_width = past_state.shape[2]
    head_shape = (own_rows, local_heads, head_width)
    floors = forget_floor.reshape(local_heads, head_width)
    forget_heads = pre_forget.reshape(head_shape)
    forget = floors + (1.0 - floors) * jax.nn.sigmoid(forget_heads)
    written = (1.0 - floors) * jax.nn.sigmoid(-forget_heads)
    query_act = jax.nn.silu(pre_query.reshape(head_shape))
    value_act = pre_value.reshape(head_shape)
    new_state = (
        forget[:, :, :, None] * past_state + written[:, :, :, None] * value_act[:, :, None, :]
    )
    readout = jnp.einsum("bhkv,bhk->bhv", new_state, query_act, precision=lax.Precision.HIGHEST)
    readout = (
        readout
        * lax.rsqrt(jnp.mean(readout * readout, axis=2, keepdims=True) + epsilon)
        * head_gain
    )
    mixed_in = (
        readout.reshape(own_rows, local_heads * head_width) * jax.nn.silu(pre_gate_out)
    ).astype(jnp.bfloat16)
    partials = jnp.dot(
        lax.all_gather(mixed_in, "kv", axis=0, tiled=True),
        proj_out,
        preferred_element_type=jnp.float32,
    ).astype(jnp.bfloat16)
    mixed_sum = lax.psum_scatter(partials, "tp", scatter_dimension=1, tiled=True).astype(
        jnp.float32
    )
    second = (after_first.astype(jnp.float32) + mixed_sum).astype(jnp.bfloat16)
    hidden_two = half_inputs(second, post_gain, post_gate, post_up)
    result = (second.astype(jnp.float32) + 0.5 * down_sum(hidden_two, post_down)).astype(
        jnp.bfloat16
    )
    return (result, new_state)


def solution(mesh):
    placed = (
        P(None, ("kv", "tp")),
        P("kv", "tp", None, None),
        P(),
        P(None, ("kv", "tp")),
        P(None, ("kv", "tp")),
        P(("kv", "tp"), None),
        P(),
        P("kv", "tp"),
        P("kv", "tp"),
        P("kv", "tp"),
        P("kv", "tp"),
        P("tp"),
        P(),
        P("tp", "kv"),
        P(),
        P(None, ("kv", "tp")),
        P(None, ("kv", "tp")),
        P(("kv", "tp"), None),
    )
    return jax.shard_map(
        per_device,
        mesh=mesh,
        in_specs=placed,
        out_specs=(P(None, ("kv", "tp")), P("kv", "tp", None, None)),
        check_vma=False,
    )
```

profile of v0, /device:TPU:0, one launch (start us, length us, event | category | flops | bytes accessed | tf_op | source)
XLA Modules:
  0.0 548.7 jit_solution(15226853268982632663)
XLA Ops:
  8.0 58.6 %all-gather.3.cloned.1.call-done = bf16[256,4096]{1,0:T(8,128)(2,1)} async-done(((bf16[256,128]{1,0:T(8,128)(2,1)}), bf16[256,4096]{1,0:T(8,128)(2,1)}) %all-gather.3.cloned.1.call-update) | async-done | bytes 2097168 | tf_op jit(solution)/shard_map/all_gather | solution.py:49
  66.6 2.1 fusion
  68.7 3.4 fusion.12
  72.1 7.5 %convolution_convert_fusion = bf16[256,4096]{1,0:T(8,128)(2,1)} fusion(bf16[352,4096]{1,0:T(8,128)(2,1)S(1)} %copy-done, bf16[4096,352]{0,1:T(8,128)(2,1)} %param.22, bf16[256,4096]{1,0:T(8,128)(2,1)} %all-gather.3.cloned.1.call-done, f32[4096]{0:T(1024)S(1)} %copy-done.7, f32[256,352]{0,1:T(8,128)S(1)} %fusion.12, f32[256]{0:T(256)S(1)} %add_rsqrt_fusion.2), kind=kOutput, calls=%fused_computation.5 | convolution fusion | flops 1481220096 | bytes 10339328 | tf_op jit(solution)/shard_map/dot_general | solution.py:57
  79.7 68.1 %reduce-scatter.7.cloned.1.call-done = bf16[256,512]{1,0:T(8,128)(2,1)} async-done(((bf16[256,4096]{1,0:T(8,128)(2,1)}), bf16[256,512]{1,0:T(8,128)(2,1)}) %reduce-scatter.7.cloned.1.call-update) | async-done | bytes 262160 | tf_op jit(solution)/shard_map/reduce_scatter | solution.py:56
  148.6 32.8 %all-reduce.2.cloned.1.call-done = bf16[256,512]{1,0:T(8,128)(2,1)} async-done(((bf16[256,512]{1,0:T(8,128)(2,1)}), bf16[256,512]{1,0:T(8,128)(2,1)}) %all-reduce.2.cloned.1.call-update) | async-done | bytes 262160 | tf_op jit(solution)/shard_map/psum | solution.py:62
  181.4 1.2 fusion.42
  182.6 1.3 convolution_convert_fusion.3
  183.9 1.3 convolution_convert_fusion.2
  185.3 1.3 convolution_convert_fusion.4
  186.6 1.3 convolution_convert_fusion.5
  189.2 21.6 %psum.15 = f32[256]{0:T(256)S(1)} all-reduce(f32[256]{0:T(256)S(1)} %get-tuple-element.2), channel_id=1, replica_groups=mesh['kv'=8,'tp'=4] {'kv'}, use_global_device_ids=true, to_apply=%region_5.6 | all-reduce | flops 256 | bytes 2048 | tf_op jit(solution)/shard_map/psum | solution.py:77
  210.8 42.6 %reduce-scatter.9.cloned.1.call-done = bf16[32,2048]{1,0:T(8,128)(2,1)} async-done(((bf16[256,2048]{1,0:T(8,128)(2,1)}), bf16[32,2048]{1,0:T(8,128)(2,1)}) %reduce-scatter.9.cloned.1.call-update) | async-done | bytes 131088 | tf_op jit(solution)/shard_map/reduce_scatter | solution.py:81
  258.2 1.5 div.63
  260.5 8.2 %multiply_add_fusion = f32[32,4,128,128]{3,2,1,0:T(8,128)S(1)} fusion(f32[32,4,128,128]{3,2,1,0:T(8,128)} %param.19, f32[32,4,128]{2,1,0:T(4,128)S(1)} %mul.203, f32[32,4,128]{2,1,0:T(4,128)S(1)} %bitcast.39, f32[32,4,128]{2,1,0:T(4,128)S(1)} %bitcast.38), kind=kLoop, calls=%fused_computation | loop fusion | flops 6291456 | bytes 16973824 | tf_op jit(solution)/shard_map/add | solution.py:106
  268.8 7.2 %fusion.65 = f32[32,4,1,128]{3,2,1,0:T(1,128)S(1)} fusion(f32[32,4,128,128]{3,2,1,0:T(8,128)S(1)} %multiply_add_fusion, f32[32,4,128,1]{2,3,1,0:T(1,128)S(1)} %bitcast.37), kind=kOutput, calls=%fused_computation.68 | convolution fusion | flops 25165824 | bytes 8519680 | tf_op jit(solution)/shard_map/bhkv,bhk->bhv/dot_general | solution.py:108
  276.3 30.8 %all_gather.10 = bf16[256,512]{1,0:T(8,128)(2,1)S(1)} all-gather(bf16[32,512]{1,0:T(8,128)(2,1)S(1)} %fusion.61), channel_id=1, replica_groups=mesh['kv'=8,'tp'=4] {'kv'}, dimensions={0}, use_global_device_ids=true | all-gather | bytes 294912 | tf_op jit(solution)/shard_map/all_gather | solution.py:118
  308.3 19.2 %reduce-scatter.13.cloned.1.call-done = bf16[128,256]{1,0:T(8,128)(2,1)} async-done(((bf16[512,256]{1,0:T(8,128)(2,1)}), bf16[128,256]{1,0:T(8,128)(2,1)}) %reduce-scatter.13.cloned.1.call-update) | async-done | bytes 65552
  329.4 54.4 %all-gather.5.cloned.1.call-done = bf16[256,4096]{1,0:T(8,128)(2,1)} async-done(((bf16[256,128]{1,0:T(8,128)(2,1)}), bf16[256,4096]{1,0:T(8,128)(2,1)}) %all-gather.5.cloned.1.call-update) | async-done | bytes 2097168 | tf_op jit(solution)/shard_map/all_gather | solution.py:11
  383.8 2.1 fusion.2
  385.9 3.4 fusion.18
  389.3 8.9 %fusion.37 = f32[256,4096]{1,0:T(8,128)} fusion(bf16[352,4096]{1,0:T(8,128)(2,1)} %param.35, bf16[4096,352]{0,1:T(8,128)(2,1)} %param.34, bf16[256,4096]{1,0:T(8,128)(2,1)} %all-gather.5.cloned.1.call-done, f32[4096]{0:T(1024)S(1)} %copy-done.4, f32[256,352]{0,1:T(8,128)S(1)} %fusion.18, f32[256]{0:T(256)S(1)} %add_rsqrt_fusion.1), kind=kOutput, calls=%fused_computation.27 | convolution fusion | flops 1480171520 | bytes 12436480 | tf_op jit(solution)/shard_map/dot_general | solution.py:22
  398.3 142.1 %reduce-scatter.11.cloned.1.call-done = f32[256,128]{1,0:T(8,128)} async-done(((f32[256,4096]{1,0:T(8,128)}), f32[256,128]{1,0:T(8,128)}) %reduce-scatter.11.cloned.1.call-update) | async-done | bytes 131088 | tf_op jit(solution)/shard_map/reduce_scatter | solution.py:21
  540.3 1.6 add_convert_fusion.1
  (53 shorter events, 11.8 us)
Async XLA Ops:
  7.2 65.0 %copy-start = (bf16[352,4096]{1,0:T(8,128)(2,1)S(1)}, bf16[352,4096]{1,0:T(8,128)(2,1)}, u32[]{:S(2)}) copy-start(bf16[352,4096]{1,0:T(8,128)(2,1)} %param.23) | copy-start | bytes 8650756
  7.2 59.4 %all-gather.3.cloned.1.call-start = ((), (), s32[]{:S(2)}) async-start(), calls=%async_computation.4 | async-start | bytes 2162688 | tf_op jit(solution)/shard_map/all_gather | solution.py:49
  7.9 139.8 %reduce-scatter.7.cloned.1.call-start = ((), (), s32[]{:S(2)}) async-start(), calls=%async_computation.5 | async-start | bytes 2359296 | tf_op jit(solution)/shard_map/reduce_scatter | solution.py:56
  68.7 3.5 copy-start.7
  79.6 101.7 %all-reduce.2.cloned.1.call-start = ((), (), s32[]{:S(2)}) async-start(), calls=%async_computation.6 | async-start | bytes 524288 | tf_op jit(solution)/shard_map/psum | solution.py:62
  147.8 105.7 %reduce-scatter.9.cloned.1.call-start = ((), (), s32[]{:S(2)}) async-start(), calls=%async_computation.7 | async-start | bytes 1179648 | tf_op jit(solution)/shard_map/reduce_scatter | solution.py:81
  185.3 3.9 copy-start.5
  189.1 138.4 %reduce-scatter.13.cloned.1.call-start = ((), (), s32[]{:S(2)}) async-start(), calls=%async_computation.10 | async-start | bytes 327680
  268.8 7.2 %copy-start.1 = (f32[32,4,128,128]{3,2,1,0:T(8,128)}, f32[32,4,128,128]{3,2,1,0:T(8,128)S(1)}, u32[]{:S(2)}) copy-start(f32[32,4,128,128]{3,2,1,0:T(8,128)S(1)} %multiply_add_fusion) | copy-start | bytes 25165828
  268.8 7.3 %copy-start.6 = (f32[128]{0:T(128)S(1)}, f32[128]{0:T(128)}, u32[]{:S(2)}) copy-start(f32[128]{0:T(128)} %param.30) | copy-start | bytes 1540
  268.8 38.3 %copy-start.3 = (bf16[512,512]{1,0:T(8,128)(2,1)S(1)}, bf16[512,512]{1,0:T(8,128)(2,1)}, u32[]{:S(2)}) copy-start(bf16[512,512]{1,0:T(8,128)(2,1)} %param.31) | copy-start | bytes 1572868
  276.0 109.9 %copy-start.4 = (f32[4096]{0:T(1024)S(1)}, f32[4096]{0:T(1024)}, u32[]{:S(2)}) copy-start(f32[4096]{0:T(1024)} %param.32) | copy-start | bytes 49156
  308.3 75.5 %all-gather.5.cloned.1.call-start = ((), (), s32[]{:S(2)}) async-start(), calls=%async_computation.8 | async-start | bytes 2162688 | tf_op jit(solution)/shard_map/all_gather | solution.py:11
  329.1 211.2 %reduce-scatter.11.cloned.1.call-start = ((), (), s32[]{:S(2)}) async-start(), calls=%async_computation.9 | async-start | bytes 4325376 | tf_op jit(solution)/shard_map/reduce_scatter | solution.py:21
  398.2 142.1 %copy-start.2 = (bf16[256,128]{1,0:T(8,128)(2,1)S(1)}, bf16[256,128]{1,0:T(8,128)(2,1)}, u32[]{:S(2)}) copy-start(bf16[256,128]{1,0:T(8,128)(2,1)} %add_convert_fusion.2) | copy-start | bytes 196612
Sparse Core Ops, SparseCore 0:
  10.8 55.6 all-gather.2
  79.7 67.9 reduce-scatter.6
  150.1 31.2 all-reduce.1
  189.2 64.1 reduce-scatter.8
  308.4 19.0 reduce-scatter.12
  330.8 52.9 all-gather.4
  398.4 141.8 reduce-scatter.10
where the time goes:
time: 550 us; the launch traced here: 549 us
  waiting for transfers between devices  418 us (76%)
  blocking collectives  52.4 us (10%)
  matrix products  36.1 us (7%)
  other arithmetic  20.7 us (4%)
  between operations  14.4 us (3%)
  local copies, waits for them, and re-layouts  6.21 us (1%)
    reduce_scatter x1, waiting for transfers between devices, down_sum(): lax.psum_scatter(jnp.dot(hidden, w_down, preferred_element_type=jnp.float...  142 us
    reduce_scatter x1, waiting for transfers between devices, per_device(): lax.psum_scatter(jnp.dot(hidden, pre_down, preferred_element_type=jnp.flo...  68.1 us
    all_gather x1, waiting for transfers between devices, per_device(): whole_rows = lax.all_gather(tokens, ('kv', 'tp'), axis=1, tiled=True)  58.6 us
    all_gather x1, waiting for transfers between devices, half_inputs(): lax.all_gather(activations, ('kv', 'tp'), axis=1, tiled=True)  54.4 us
    reduce_scatter x1, waiting for transfers between devices, per_device(): lax.psum_scatter(jnp.concatenate([jnp.dot(normed, weight_part, preferred_...  42.6 us
    psum x1, waiting for transfers between devices, per_device(): block_sum = lax.psum(kv_sums, 'tp').astype(jnp.float32)  32.8 us
    all_gather x1, blocking collectives, per_device(): lax.all_gather(mixed_in, 'kv', axis=0, tiled=True)  30.8 us
    psum x1, blocking collectives, per_device(): squares = lax.psum(jnp.sum(block_float * block_float, axis=1), 'kv')  21.6 us
  transfers between devices with their start and end apart: 7, of which 7 were waited for; matrix products, arithmetic and copies ran while one was open for 0% of the time, Pallas kernels for 0%

commit v1 on v0

--- a/solution.py
+++ b/solution.py
@@ -46,7 +46,7 @@
     post_up,
     post_down,
 ):
-    whole_rows = lax.all_gather(tokens, ("kv", "tp"), axis=1, tiled=True)
+    whole_rows = jnp.concatenate(lax.all_gather(tokens, ("kv", "tp")), axis=1)
     whole_float = whole_rows.astype(jnp.float32)
     row_scale = lax.rsqrt(jnp.mean(whole_float * whole_float, axis=1, keepdims=True) + epsilon)
     normed = (whole_float * pre_gain).astype(jnp.bfloat16)

time: 550 us -> 554 us (level)
  local copies, waits for them, and re-layouts: 6.21 us -> 12.9 us
  transfers between devices with their start and end apart: 7 -> 7, of which waited for: 7 -> 7; matrix products, arithmetic and copies ran while one was open for 0% -> 1% of each run, Pallas kernels for 0% -> 0%
where the time goes in v1:
time: 554 us; the launch traced here: 553 us
  waiting for transfers between devices  418 us (75%)
  blocking collectives  52.5 us (9%)
  matrix products  33 us (6%)
  other arithmetic  22.2 us (4%)
  between operations  14.4 us (3%)
  local copies, waits for them, and re-layouts  12.9 us (2%)
    reduce_scatter x1, waiting for transfers between devices, down_sum(): lax.psum_scatter(jnp.dot(hidden, w_down, preferred_element_type=jnp.float...  142 us
    reduce_scatter x1, waiting for transfers between devices, per_device(): lax.psum_scatter(jnp.dot(hidden, pre_down, preferred_element_type=jnp.flo...  67.9 us
    all_gather x1, waiting for transfers between devices, per_device(): whole_rows = jnp.concatenate(lax.all_gather(tokens, ('kv', 'tp')), axis=1)  61.8 us
    all_gather x1, waiting for transfers between devices, half_inputs(): lax.all_gather(activations, ('kv', 'tp'), axis=1, tiled=True)  54.4 us
    reduce_scatter x1, waiting for transfers between devices, per_device(): lax.psum_scatter(jnp.concatenate([jnp.dot(normed, weight_part, preferred_...  42.6 us
    all_gather x1, blocking collectives, per_device(): lax.all_gather(mixed_in, 'kv', axis=0, tiled=True)  30.9 us
    psum x1, waiting for transfers between devices, per_device(): block_sum = lax.psum(kv_sums, 'tp').astype(jnp.float32)  28.9 us
    psum x1, blocking collectives, per_device(): squares = lax.psum(jnp.sum(block_float * block_float, axis=1), 'kv')  21.6 us
  transfers between devices with their start and end apart: 7, of which 7 were waited for; matrix products, arithmetic and copies ran while one was open for 1% of the time, Pallas kernels for 0%

profile of v1, /device:TPU:0, one launch (start us, length us, event | category | flops | bytes accessed | tf_op | source)
XLA Modules:
  0.0 553.1 jit_solution(11359648333969376564)
XLA Ops:
  8.0 61.8 %all-gather.6.cloned.1.call-done = bf16[8192,128]{1,0:T(8,128)(2,1)} async-done(((bf16[256,128]{1,0:T(8,128)(2,1)}), bf16[8192,128]{1,0:T(8,128)(2,1)}) %all-gather.6.cloned.1.call-update) | async-done | bytes 2097168 | tf_op jit(solution)/shard_map/all_gather | solution.py:49
  69.8 3.5 multiply_reduce_fusion
  73.3 1.4 copy.21
  76.0 1.3 fusion.14
  77.4 7.5 %convolution_convert_fusion = bf16[256,4096]{1,0:T(8,128)(2,1)} fusion(bf16[352,4096]{1,0:T(8,128)(2,1)S(1)} %copy-done, bf16[4096,352]{0,1:T(8,128)(2,1)} %param.22, f32[4096]{0:T(1024)S(1)} %copy-done.11, f32[256,352]{0,1:T(8,128)S(1)} %fusion.14, f32[256]{0:T(256)S(1)} %add_rsqrt_fusion.2, bf16[32,8,32,128]{3,2,1,0:T(8,128)(2,1)} %bitcast.49), kind=kOutput, calls=%fused_computation.3 | convolution fusion | flops 1481220096 | bytes 10339328 | tf_op jit(solution)/shard_map/dot_general | solution.py:57
  84.9 67.9 %reduce-scatter.7.cloned.1.call-done = bf16[256,512]{1,0:T(8,128)(2,1)} async-done(((bf16[256,4096]{1,0:T(8,128)(2,1)}), bf16[256,512]{1,0:T(8,128)(2,1)}) %reduce-scatter.7.cloned.1.call-update) | async-done | bytes 262160 | tf_op jit(solution)/shard_map/reduce_scatter | solution.py:56
  153.6 3.9 copy.38
  157.6 28.9 %all-reduce.2.cloned.1.call-done = bf16[256,512]{1,0:T(8,128)(2,1)} async-done(((bf16[256,512]{1,0:T(8,128)(2,1)}), bf16[256,512]{1,0:T(8,128)(2,1)}) %all-reduce.2.cloned.1.call-update) | async-done | bytes 262160 | tf_op jit(solution)/shard_map/psum | solution.py:62
  187.8 1.3 convolution_convert_fusion.3
  189.1 1.3 convolution_convert_fusion.2
  190.5 1.4 convolution_convert_fusion.4
  193.4 21.6 %psum.15 = f32[256]{0:T(256)S(1)} all-reduce(f32[256]{0:T(256)S(1)} %get-tuple-element.2), channel_id=1, replica_groups=mesh['kv'=8,'tp'=4] {'kv'}, use_global_device_ids=true, to_apply=%region_5.6 | all-reduce | flops 256 | bytes 2048 | tf_op jit(solution)/shard_map/psum | solution.py:77
  215.1 42.6 %reduce-scatter.9.cloned.1.call-done = bf16[32,2048]{1,0:T(8,128)(2,1)} async-done(((bf16[256,2048]{1,0:T(8,128)(2,1)}), bf16[32,2048]{1,0:T(8,128)(2,1)}) %reduce-scatter.9.cloned.1.call-update) | async-done | bytes 131088 | tf_op jit(solution)/shard_map/reduce_scatter | solution.py:81
  262.4 1.5 div.63
  264.8 8.2 %multiply_add_fusion = f32[32,4,128,128]{3,2,1,0:T(8,128)S(1)} fusion(f32[32,4,128,128]{3,2,1,0:T(8,128)} %param.19, f32[32,4,128]{2,1,0:T(4,128)S(1)} %mul.204, f32[32,4,128]{2,1,0:T(4,128)S(1)} %bitcast.59, f32[32,4,128]{2,1,0:T(4,128)S(1)} %bitcast.58), kind=kLoop, calls=%fused_computation | loop fusion | flops 6291456 | bytes 16973824 | tf_op jit(solution)/shard_map/add | solution.py:106
  273.1 7.2 %fusion.51 = f32[32,4,1,128]{3,2,1,0:T(1,128)S(1)} fusion(f32[32,4,128,128]{3,2,1,0:T(8,128)S(1)} %multiply_add_fusion, f32[32,4,128,1]{2,3,1,0:T(1,128)S(1)} %bitcast.57), kind=kOutput, calls=%fused_computation.67 | convolution fusion | flops 25165824 | bytes 8519680 | tf_op jit(solution)/shard_map/bhkv,bhk->bhv/dot_general | solution.py:108
  280.6 30.9 %all_gather.14 = bf16[256,512]{1,0:T(8,128)(2,1)S(1)} all-gather(bf16[32,512]{1,0:T(8,128)(2,1)S(1)} %fusion.47), channel_id=1, replica_groups=mesh['kv'=8,'tp'=4] {'kv'}, dimensions={0}, use_global_device_ids=true | all-gather | bytes 294912 | tf_op jit(solution)/shard_map/all_gather | solution.py:118
  312.7 18.8 %reduce-scatter.13.cloned.1.call-done = bf16[128,256]{1,0:T(8,128)(2,1)} async-done(((bf16[512,256]{1,0:T(8,128)(2,1)}), bf16[128,256]{1,0:T(8,128)(2,1)}) %reduce-scatter.13.cloned.1.call-update) | async-done | bytes 65552
  333.4 54.4 %all-gather.4.cloned.1.call-done = bf16[256,4096]{1,0:T(8,128)(2,1)} async-done(((bf16[256,128]{1,0:T(8,128)(2,1)}), bf16[256,4096]{1,0:T(8,128)(2,1)}) %all-gather.4.cloned.1.call-update) | async-done | bytes 2097168 | tf_op jit(solution)/shard_map/all_gather | solution.py:11
  387.8 2.1 fusion
  389.9 3.4 fusion.8
  393.3 9.0 %fusion.25 = f32[256,4096]{1,0:T(8,128)} fusion(bf16[352,4096]{1,0:T(8,128)(2,1)} %param.35, bf16[4096,352]{0,1:T(8,128)(2,1)} %param.34, bf16[256,4096]{1,0:T(8,128)(2,1)} %all-gather.4.cloned.1.call-done, f32[4096]{0:T(1024)S(1)} %copy-done.7, f32[256,352]{0,1:T(8,128)S(1)} %fusion.8, f32[256]{0:T(256)S(1)} %add_rsqrt_fusion.1), kind=kOutput, calls=%fused_computation.26 | convolution fusion | flops 1480171520 | bytes 12436480 | tf_op jit(solution)/shard_map/dot_general | solution.py:22
  402.3 142.4 %reduce-scatter.11.cloned.1.call-done = f32[256,128]{1,0:T(8,128)} async-done(((f32[256,4096]{1,0:T(8,128)}), f32[256,128]{1,0:T(8,128)}) %reduce-scatter.11.cloned.1.call-update) | async-done | bytes 131088 | tf_op jit(solution)/shard_map/reduce_scatter | solution.py:21
  544.7 1.6 add_convert_fusion.1
  (63 shorter events, 14.8 us)
Async XLA Ops:
  7.2 70.2 %copy-start = (bf16[352,4096]{1,0:T(8,128)(2,1)S(1)}, bf16[352,4096]{1,0:T(8,128)(2,1)}, u32[]{:S(2)}) copy-start(bf16[352,4096]{1,0:T(8,128)(2,1)} %param.23) | copy-start | bytes 8650756
  7.2 62.6 %all-gather.6.cloned.1.call-start = ((), (), s32[]{:S(2)}) async-start(), calls=%async_computation.9 | async-start | bytes 2162688 | tf_op jit(solution)/shard_map/all_gather | solution.py:49
  7.9 144.9 %reduce-scatter.7.cloned.1.call-start = ((), (), s32[]{:S(2)}) async-start(), calls=%async_computation.4 | async-start | bytes 2359296 | tf_op jit(solution)/shard_map/reduce_scatter | solution.py:56
  69.8 3.5 copy-start.3
  69.8 6.2 %copy-start.10 = (bf16[4096,352]{0,1:T(8,128)(2,1)S(1)}, bf16[4096,352]{0,1:T(8,128)(2,1)}, u32[]{:S(2)}) copy-start(bf16[4096,352]{0,1:T(8,128)(2,1)} %param.21) | copy-start | bytes 8650756
  69.8 6.2 %copy-start.11 = (f32[4096]{0:T(1024)S(1)}, f32[4096]{0:T(1024)}, u32[]{:S(2)}) copy-start(f32[4096]{0:T(1024)} %param.20) | copy-start | bytes 49156
  74.7 1.3 copy-start.2
  84.9 101.6 %all-reduce.2.cloned.1.call-start = ((), (), s32[]{:S(2)}) async-start(), calls=%async_computation.5 | async-start | bytes 524288 | tf_op jit(solution)/shard_map/psum | solution.py:62
  152.8 104.9 %reduce-scatter.9.cloned.1.call-start = ((), (), s32[]{:S(2)}) async-start(), calls=%async_computation.6 | async-start | bytes 1179648 | tf_op jit(solution)/shard_map/reduce_scatter | solution.py:81
  186.5 5.4 copy-start.5
  190.5 2.9 copy-start.8
  193.3 138.1 %reduce-scatter.13.cloned.1.call-start = ((), (), s32[]{:S(2)}) async-start(), calls=%async_computation.10 | async-start | bytes 327680
  273.0 7.2 %copy-start.1 = (f32[32,4,128,128]{3,2,1,0:T(8,128)}, f32[32,4,128,128]{3,2,1,0:T(8,128)S(1)}, u32[]{:S(2)}) copy-start(f32[32,4,128,128]{3,2,1,0:T(8,128)S(1)} %multiply_add_fusion) | copy-start | bytes 25165828
  273.0 7.3 %copy-start.9 = (f32[128]{0:T(128)S(1)}, f32[128]{0:T(128)}, u32[]{:S(2)}) copy-start(f32[128]{0:T(128)} %param.30) | copy-start | bytes 1540
  273.1 38.4 %copy-start.6 = (bf16[512,512]{1,0:T(8,128)(2,1)S(1)}, bf16[512,512]{1,0:T(8,128)(2,1)}, u32[]{:S(2)}) copy-start(bf16[512,512]{1,0:T(8,128)(2,1)} %param.31) | copy-start | bytes 1572868
  280.3 109.6 %copy-start.7 = (f32[4096]{0:T(1024)S(1)}, f32[4096]{0:T(1024)}, u32[]{:S(2)}) copy-start(f32[4096]{0:T(1024)} %param.32) | copy-start | bytes 49156
  312.6 75.1 %all-gather.4.cloned.1.call-start = ((), (), s32[]{:S(2)}) async-start(), calls=%async_computation.7 | async-start | bytes 2162688 | tf_op jit(solution)/shard_map/all_gather | solution.py:11
  333.1 211.6 %reduce-scatter.11.cloned.1.call-start = ((), (), s32[]{:S(2)}) async-start(), calls=%async_computation.8 | async-start | bytes 4325376 | tf_op jit(solution)/shard_map/reduce_scatter | solution.py:21
  402.2 142.4 %copy-start.4 = (bf16[256,128]{1,0:T(8,128)(2,1)S(1)}, bf16[256,128]{1,0:T(8,128)(2,1)}, u32[]{:S(2)}) copy-start(bf16[256,128]{1,0:T(8,128)(2,1)} %add_convert_fusion.2) | copy-start | bytes 196612
Sparse Core Ops, SparseCore 0:
  10.8 58.9 all-gather.5
  85.0 67.7 reduce-scatter.6
  155.1 31.3 all-reduce.1
  193.4 64.2 reduce-scatter.8
  312.8 18.6 reduce-scatter.12
  334.7 52.9 all-gather.3
  402.4 142.2 reduce-scatter.10
